TPU v7x, 32 devices: a whole 2x2x4 slice. The times are simulated.
32 devices in a mesh: sp: 4 (over z), tp: 2 (over y), dp: 4 (over x, core).
Axes of the slice: x: 2, y: 2, z: 4, core: 2. Of those that a mesh axis runs over, the one named last changes fastest.
Arguments:
- latent: bfloat16 [2048, 2048], P(('dp', 'sp', 'tp')), parts along dimension 0, may hold values from -6 to 6
- cond: bfloat16 [8192], P('dp'), parts along dimension 0, may hold values from -6 to 6
- context: bfloat16 [2048, 2048], P(('dp', 'sp')), parts along dimension 0, may hold values from -6 to 6
- context_cond: bfloat16 [2048], replicated, may hold values from -6 to 6
- modulation: bfloat16 [2048, 6144], P(('sp', 'tp')), may hold values from -0.125 to 0.125
- norm_gain: bfloat16 [2048], replicated, may hold values from 0.099609375 to 1.8984375
- w_x: bfloat16 [2048, 1024], P(None, 'tp'), may hold values from -0.125 to 0.125
- w_gate: bfloat16 [2048, 1024], P(None, 'tp'), may hold values from -0.125 to 0.125
- w_b: bfloat16 [2048, 256], P(None, 'tp'), may hold values from -0.125 to 0.125
- w_c: bfloat16 [2048, 256], P(None, 'tp'), may hold values from -0.125 to 0.125
- w_dt: bfloat16 [2, 2048, 16], P(None, None, 'tp'), may hold values from -0.125 to 0.125
- conv_x: bfloat16 [4, 1024], P(None, 'tp'), may hold values from -3 to 3
- conv_b: bfloat16 [4, 256], P(None, 'tp'), may hold values from -3 to 3
- conv_c: bfloat16 [4, 256], P(None, 'tp'), may hold values from -3 to 3
- decay_rate: float32 [2, 16], P(None, 'tp'), may hold values from 0 to 0.04
- decay_extra: float32 [2048, 16], P(('dp', 'sp'), 'tp'), parts along dimension 0, may hold values from -2 to 0
- out_gain: bfloat16 [1024], P('tp'), may hold values from 0.099609375 to 1.8984375
- w_out: bfloat16 [1024, 2048], replicated, may hold values from -0.1875 to 0.1875
Outputs:
- mixed: bfloat16 [2048, 2048], P(('dp', 'sp', 'tp')), parts along dimension 0
There are 4 independent parts, one for each index of `dp`. A program takes and returns all parts, laid end to end along the dimension named above; an argument that names none is the same for every part. Nothing has to cross between parts.
All inputs are finite; a program needn't handle non-finite values.
Results may differ from a plain program's by a relative error of at most 0.007.
Values may be sent and summed in bfloat16 or wider, within the bound.
A program may use at most 64 MiB of HBM per device.

v0:
```python
import jax
import jax.numpy as jnp
from jax import lax
from jax.sharding import PartitionSpec as P

HEAD_DIM = 64
STATE = 64
BLOCK = 128
ROW_EPS = 1e-06
GROUP_EPS = 1e-05
HIGHEST = lax.Precision.HIGHEST


def prefix(x, axis, join, neutral, backward):
    count = lax.axis_size(axis)
    place = lax.axis_index(axis)
    ahead = count - 1 - place if backward else place
    gathered = jax.tree.map(
        lambda a, kind: lax.all_gather(a.astype(kind), axis),
        x,
        jax.tree.map(lambda a: jnp.bfloat16 if a.dtype == jnp.float32 else a.dtype, x),
    )
    state = jax.tree.map(lambda a, e: jnp.zeros_like(a) + jnp.asarray(e, a.dtype), x, neutral)

    def one(hop, state):
        source = count - 1 - hop if backward else hop
        return join(
            state,
            jax.tree.map(
                lambda a, own: lax.dynamic_index_in_dim(a, source, 0, False).astype(own.dtype),
                gathered,
                x,
            ),
        )

    return lax.fori_loop(0, ahead, one, state)


def with_halo(block, sides, width):
    for axis, dim in sides:
        count = lax.axis_size(axis)
        forward = [(i, i + 1) for i in range(count - 1)]
        backward = [(target, source) for source, target in forward]
        low = lax.ppermute(
            lax.slice_in_dim(block, block.shape[dim] - width, None, axis=dim), axis, forward
        )
        high = lax.ppermute(lax.slice_in_dim(block, 0, width, axis=dim), axis, backward)
        block = jnp.concatenate([low, block, high], axis=dim)
    return block


def modulated_norm(row_block, norm_gain, shift_row, scale_row):
    values = row_block.astype(jnp.float32)
    normed = values * lax.rsqrt(jnp.mean(values * values, axis=-1, keepdims=True) + ROW_EPS)
    return (normed * norm_gain.astype(jnp.float32) * (1.0 + scale_row) + shift_row).astype(
        jnp.bfloat16
    )


def project_many(row_block, weights):
    return jnp.concatenate(
        [
            jnp.dot(row_block, weight, preferred_element_type=jnp.float32).astype(jnp.bfloat16)
            for weight in weights
        ],
        axis=1,
    )


def conv_padded(padded, conv_taps, length):
    values = padded.astype(jnp.float32)
    summed = jnp.zeros((length, values.shape[1]), jnp.float32)
    for offset in range(conv_taps.shape[0]):
        summed = summed + conv_taps[offset].astype(jnp.float32) * values[offset : offset + length]
    return jax.nn.silu(summed).astype(jnp.bfloat16)


def context_states(ctx_xs, ctx_bmat, ctx_dt, decay_rate):
    length = ctx_xs.shape[0]
    groups = ctx_bmat.shape[1] // STATE
    heads_here = ctx_dt.shape[2]
    repeat = heads_here // groups
    values = ctx_xs.astype(jnp.float32).reshape(length, groups, repeat, HEAD_DIM)
    keys_b = ctx_bmat.astype(jnp.float32).reshape(length, groups, STATE)
    log_decay = -decay_rate[:, None, :] * ctx_dt
    running = jnp.cumsum(log_decay, axis=1)
    forward_weight = (jnp.exp(running[0, -1:] - running[0]) * ctx_dt[0]).reshape(
        length, groups, repeat
    )
    backward_weight = (jnp.exp(running[1] - log_decay[1]) * ctx_dt[1]).reshape(
        length, groups, repeat
    )
    forward_state = jnp.einsum(
        "lgn,lgr,lgrp->grpn", keys_b, forward_weight, values, precision=HIGHEST
    )
    backward_state = jnp.einsum(
        "lgn,lgr,lgrp->grpn", keys_b, backward_weight, values, precision=HIGHEST
    )
    return (forward_state, backward_state)


def block_pass(inputs, step_sizes, log_decay, bmat, cmat, start_state):
    length = inputs.shape[0]
    groups, repeat = (start_state.shape[0], start_state.shape[1])
    block_count = length // BLOCK
    values = inputs.reshape(block_count, BLOCK, groups, repeat, HEAD_DIM)
    steps_blk = step_sizes.reshape(block_count, BLOCK, groups, repeat)
    decays = log_decay.reshape(block_count, BLOCK, groups, repeat)
    keys_b = bmat.reshape(block_count, BLOCK, groups, STATE)
    reads_c = cmat.reshape(block_count, BLOCK, groups, STATE)
    lower_mask = (jnp.arange(BLOCK)[:, None] >= jnp.arange(BLOCK)[None, :])[:, :, None, None]

    def advance(carried, block_data):
        value_blk, step_blk, decay_blk, key_blk, read_blk = block_data
        running = jnp.cumsum(decay_blk, axis=0)
        log_gaps = running[:, None] - running[None, :]
        mixing = jnp.where(lower_mask, jnp.exp(jnp.where(lower_mask, log_gaps, 0.0)), 0.0)
        affinity = jnp.einsum("ign,jgn->ijg", read_blk, key_blk, preferred_element_type=jnp.float32)
        weights = (affinity[..., None] * mixing * step_blk[None]).astype(jnp.bfloat16)
        output = jnp.einsum(
            "ijgr,jgrp->igrp", weights, value_blk, preferred_element_type=jnp.float32
        )
        output = output + jnp.einsum(
            "ign,grpn,igr->igrp",
            read_blk.astype(jnp.float32),
            carried,
            jnp.exp(running),
            precision=HIGHEST,
        )
        to_end = jnp.exp(running[-1:] - running) * step_blk
        state_in = (key_blk.astype(jnp.float32)[:, :, None, :] * to_end[..., None]).astype(
            jnp.bfloat16
        )
        carried = jnp.exp(running[-1])[..., None, None] * carried + jnp.einsum(
            "jgrn,jgrp->grpn", state_in, value_blk, preferred_element_type=jnp.float32
        )
        return (carried, output)

    final_state, outputs = lax.scan(
        advance, start_state, (values, steps_blk, decays, keys_b, reads_c)
    )
    return (outputs.reshape(length, groups, repeat, HEAD_DIM), final_state)


def state_chain(summary, backward):

    def combine(earlier, later_part):
        return (
            earlier[0] + later_part[0],
            jnp.exp(later_part[0])[..., None, None] * earlier[1] + later_part[1],
        )

    identity_pair = (jnp.zeros_like(summary[0]), jnp.zeros_like(summary[1]))
    return prefix(summary, "sp", combine, identity_pair, backward)


def directed_pass(inputs, step_sizes, log_decay, bmat, cmat, outer_start, zeros_state, backward):
    local_out, final_state = block_pass(inputs, step_sizes, log_decay, bmat, cmat, zeros_state)
    length = inputs.shape[0]
    groups, repeat = (zeros_state.shape[0], zeros_state.shape[1])
    running = jnp.cumsum(log_decay, axis=0).reshape(length, groups, repeat)
    before = state_chain((running[-1], final_state), backward)
    entry_state = jnp.exp(before[0])[..., None, None] * outer_start + before[1]
    read_rows = cmat.astype(jnp.float32).reshape(length, groups, STATE)
    return local_out + jnp.einsum(
        "tgn,grpn,tgr->tgrp", read_rows, entry_state, jnp.exp(running), precision=HIGHEST
    )


def group_norm(combined, out_gain):
    length, groups, repeat, _ = combined.shape
    mean_square = jnp.mean(combined * combined, axis=(2, 3), keepdims=True)
    scaled = (
        combined
        * lax.rsqrt(mean_square + GROUP_EPS)
        * out_gain.astype(jnp.float32).reshape(groups, repeat, HEAD_DIM)
    )
    return scaled.reshape(length, groups * repeat * HEAD_DIM).astype(jnp.bfloat16)


def local(
    latent,
    cond,
    context,
    context_cond,
    modulation,
    norm_gain,
    w_x,
    w_gate,
    w_b,
    w_c,
    w_dt,
    conv_x,
    conv_b,
    conv_c,
    decay_rate,
    decay_extra,
    out_gain,
    w_out,
):
    model_width = latent.shape[1]
    mod_share = modulation.shape[0]
    cond_rows = jax.nn.silu(jnp.stack([cond, context_cond]).astype(jnp.float32)).astype(
        jnp.bfloat16
    )
    own_cols = lax.dynamic_slice_in_dim(
        cond_rows, lax.axis_index(("sp", "tp")) * mod_share, mod_share, 1
    )
    mod_rows = lax.psum(
        jnp.dot(own_cols, modulation, preferred_element_type=jnp.float32), ("sp", "tp")
    )
    shift_rows = mod_rows[:, :model_width]
    scale_rows = mod_rows[:, model_width : 2 * model_width]
    gate_row = mod_rows[0, 2 * model_width :]
    head_cols = w_x.shape[1]
    state_cols = w_b.shape[1]
    heads_here = w_dt.shape[2]
    groups_here = state_cols // STATE
    repeat = heads_here // groups_here
    hidden = modulated_norm(latent, norm_gain, shift_rows[0], scale_rows[0])
    latent_mats = (w_x, w_b, w_c, w_gate, w_dt[0], w_dt[1])
    projected = project_many(lax.all_gather(hidden, "tp", axis=0, tiled=True), latent_mats)
    token_count = projected.shape[0]
    conv_cols = head_cols + 2 * state_cols
    extended = with_halo(projected[:, :conv_cols], (("sp", 0),), 2)
    conv_taps = jnp.concatenate([conv_x, conv_b, conv_c], axis=1)
    convolved = conv_padded(extended, conv_taps, token_count)
    latent_xs = convolved[:, :head_cols]
    latent_b = convolved[:, head_cols : head_cols + state_cols]
    latent_c = convolved[:, head_cols + state_cols :]
    gate_in = projected[:, conv_cols : conv_cols + head_cols]
    dt_start = conv_cols + head_cols
    latent_dt = jnp.stack(
        [
            jax.nn.softplus(projected[:, dt_start : dt_start + heads_here].astype(jnp.float32)),
            jax.nn.softplus(projected[:, dt_start + heads_here :].astype(jnp.float32)),
        ]
    )
    context_mats = (w_x, w_b, w_dt[0], w_dt[1])
    own_context = project_many(
        modulated_norm(context, norm_gain, shift_rows[1], scale_rows[1]), context_mats
    )
    context_cols = lax.all_gather(own_context, "sp", axis=0, tiled=True)
    ctx_span = head_cols + state_cols
    ctx_padded = jnp.pad(context_cols[:, :ctx_span], ((2, 1), (0, 0)))
    ctx_conv = conv_padded(
        ctx_padded, jnp.concatenate([conv_x, conv_b], axis=1), context_cols.shape[0]
    )
    ctx_dt = jnp.stack(
        [
            jax.nn.softplus(context_cols[:, ctx_span : ctx_span + heads_here].astype(jnp.float32)),
            jax.nn.softplus(context_cols[:, ctx_span + heads_here :].astype(jnp.float32)),
        ]
    )
    forward_start, backward_start = context_states(
        ctx_conv[:, :head_cols], ctx_conv[:, head_cols:], ctx_dt, decay_rate
    )
    log_decay = -decay_rate[:, None, :] * latent_dt + decay_extra[None]
    zeros_state = jnp.zeros((groups_here, repeat, HEAD_DIM, STATE), jnp.float32)
    y_forward = directed_pass(
        latent_xs, latent_dt[0], log_decay[0], latent_b, latent_c, forward_start, zeros_state, False
    )
    y_backward = directed_pass(
        latent_xs[::-1],
        latent_dt[1][::-1],
        log_decay[1][::-1],
        latent_b[::-1],
        latent_c[::-1],
        backward_start,
        zeros_state,
        True,
    )
    gate_act = jax.nn.silu(gate_in.astype(jnp.float32)).reshape(
        token_count, groups_here, repeat, HEAD_DIM
    )
    combined = (y_forward + y_backward[::-1]) * gate_act
    normed = group_norm(combined, out_gain)
    tp_count = lax.axis_size("tp")
    stacked = normed.reshape(tp_count, token_count // tp_count, normed.shape[1])
    branch = jnp.dot(
        lax.all_to_all(stacked, "tp", split_axis=0, concat_axis=2, tiled=True)[0],
        w_out,
        preferred_element_type=jnp.float32,
    )[None]
    return (latent.astype(jnp.float32) + gate_row * branch[0]).astype(jnp.bfloat16)


def solution(mesh):
    in_specs = (
        P(("dp", "sp", "tp"), None),
        P("dp"),
        P(("dp", "sp"), None),
        P(),
        P(("sp", "tp"), None),
        P(),
        P(None, "tp"),
        P(None, "tp"),
        P(None, "tp"),
        P(None, "tp"),
        P(None, None, "tp"),
        P(None, "tp"),
        P(None, "tp"),
        P(None, "tp"),
        P(None, "tp"),
        P(("dp", "sp"), "tp"),
        P("tp"),
        P(),
    )
    out_specs = P(("dp", "sp", "tp"), None)
    return jax.shard_map(local, mesh=mesh, in_specs=in_specs, out_specs=out_specs, check_vma=False)
```

profile of v0, /device:TPU:0, one launch (start us, length us, event | category | flops | bytes accessed | tf_op | source)
XLA Modules:
  0.0 247.8 jit_solution(15845269503590403432)
XLA Ops:
  2.4 39.4 %psum.7 = f32[2,6144]{1,0:T(2,128)S(1)} all-reduce(f32[2,6144]{1,0:T(2,128)S(1)} %fusion.93), channel_id=1, replica_groups=mesh['sp'=4,'tp'=2,'dp'=4] {'sp','tp'}, use_global_device_ids=true, to_apply=%region_0.1 | all-reduce | flops 12288 | bytes 98304 | tf_op jit(solution)/shard_map/psum | solution.py:209
  42.9 7.2 %all_gather.26 = bf16[128,2048]{1,0:T(8,128)(2,1)S(1)} all-gather(bf16[64,2048]{1,0:T(8,128)(2,1)S(1)} %fusion.31), channel_id=1, replica_groups=mesh['sp'=4,'tp'=2,'dp'=4] {'tp'}, dimensions={0}, use_global_device_ids=true | all-gather | bytes 786432 | tf_op jit(solution)/shard_map/all_gather | solution.py:222
  50.0 2.3 convolution_convert_fusion.2
  53.6 1.9 collective-permute-start
  55.4 1.3 collective-permute-start.1
  59.4 1.2 fusion.22
  60.7 2.9 %convolution_convert_fusion.1 = bf16[128,512]{0,1:T(8,128)(2,1)S(1)} fusion(bf16[2048,512]{1,0:T(8,128)(2,1)} %param.28, bf16[128,2048]{1,0:T(8,128)(2,1)} %param.24, f32[2048]{0:T(1024)} %bitcast.249, f32[2048]{0:T(1024)} %bitcast.253, f32[2048]{0:T(1024)S(1)} %convert_element_type.221, f32[128]{0:T(128)S(1)} %add_rsqrt_fusion.1), kind=kOutput, calls=%fused_computation.49 | convolution fusion | flops 270073856 | bytes 2777600 | tf_op jit(solution)/shard_map/dot_general | solution.py:63
  65.2 14.5 %all_gather.30 = bf16[512,656]{0,1:T(8,128)(2,1)S(1)} all-gather(bf16[128,656]{0,1:T(8,128)(2,1)S(1)} %pad_maximum_fusion), channel_id=1, replica_groups=mesh['sp'=4,'tp'=2,'dp'=4] {'sp'}, dimensions={0}, use_global_device_ids=true | all-gather | bytes 839680 | tf_op jit(solution)/shard_map/all_gather | solution.py:243
  83.7 1.0 fusion.114
  90.8 1.6 reduce_window_sum.52
  93.7 5.0 %reduce-window.6 = f32[2,8,4,128]{3,1,2,0:T(8,128)} reduce-window(f32[2,8,4,128]{3,1,2,0:T(8,128)} %fusion.148, f32[]{:T(128)} %constant.128.clone.1), window={size=1x1x1x128 pad=0_0x0_0x0_0x127_0}, to_apply=%region_7.8 | reduce-window | flops 1040384 | bytes 65540 | tf_op jit(solution)/shard_map/reduce-window
  98.7 1.5 slice_reduce_fusion
  103.1 2.7 %pad_convert_fusion = f32[515,640]{0,1:T(8,128)} fusion(bf16[512,640]{0,1:T(8,128)(2,1)} %slice.222), kind=kLoop, calls=%fused_computation.67 | loop fusion | flops 329600 | bytes 1973760 | tf_op jit(solution)/shard_map/convert_element_type | solution.py:71
  107.2 1.6 reduce_window_sum.56
  110.2 3.1 %divide_multiply_fusion = f32[128,512]{1,0:T(8,128)} fusion(bf16[128,2048]{1,0:T(8,128)(2,1)} %copy-done.2, bf16[2048,512]{1,0:T(8,128)(2,1)} %param.29), kind=kOutput, calls=%fused_computation.89 | convolution fusion | flops 268828672 | bytes 2883584 | tf_op jit(solution)/shard_map/dot_general | solution.py:63
  113.3 1.4 fusion.76
  116.3 2.4 multiply_convert_fusion
  118.7 10.4 %all_gather.27 = bf16[4,2,4]{2,1,0:T(2,128)(2,1)} all-gather(bf16[1,2,4]{2,1,0:T(2,128)(2,1)S(1)} %copy-done.55), channel_id=1, replica_groups=mesh['sp'=4,'tp'=2,'dp'=4] {'sp'}, dimensions={0}, use_global_device_ids=true | all-gather | bytes 80 | tf_op jit(solution)/shard_map/all_gather | solution.py:19
  129.1 8.0 %all_gather.31 = bf16[4,2,4]{2,1,0:T(2,128)(2,1)} all-gather(bf16[1,2,4]{2,1,0:T(2,128)(2,1)S(1)} %copy-done.56), channel_id=1, replica_groups=mesh['sp'=4,'tp'=2,'dp'=4] {'sp'}, dimensions={0}, use_global_device_ids=true | all-gather | bytes 80 | tf_op jit(solution)/shard_map/all_gather | solution.py:19
  137.1 1.9 slice.230
  139.0 1.6 slice.231
  140.5 1.5 exp.128
  142.0 1.5 exp.139
  144.9 1.0 copy.176
  145.8 1.4 reshape.201
  147.2 1.5 copy.174
  148.7 1.3 reshape.203
  150.0 1.6 copy.189
  151.6 1.5 copy.187
  153.1 1.6 copy.185
  154.6 1.6 copy.172
  156.2 1.8 copy.190
  158.0 1.3 reshape.218
  160.6 1.3 rev.18
  164.3 16.6 %all-gather = bf16[8,4,64,64]{3,2,1,0:T(8,128)(2,1)} all-gather(bf16[2,4,64,64]{3,2,1,0:T(8,128)(2,1)S(1)} %fusion.17), channel_id=2, replica_groups=mesh['sp'=4,'tp'=2,'dp'=4] {'sp'}, dimensions={0}, use_global_device_ids=true | all-gather | bytes 327680 | tf_op jit(solution)/shard_map/all_gather | solution.py:19
  181.5 1.2 exp.132
  182.7 1.6 copy.178
  184.3 1.5 copy.179
  186.6 1.1 fusion.18
  187.7 19.2 %all-gather.1 = bf16[8,4,64,64]{3,2,1,0:T(8,128)(2,1)} all-gather(bf16[2,4,64,64]{3,2,1,0:T(8,128)(2,1)S(1)} %fusion.18), channel_id=3, replica_groups=mesh['sp'=4,'tp'=2,'dp'=4] {'sp'}, dimensions={0}, use_global_device_ids=true | all-gather | bytes 327680 | tf_op jit(solution)/shard_map/all_gather | solution.py:19
  207.5 7.0 %while.7 = (s32[]{:T(128)}, f32[2,4]{1,0:T(2,128)}, f32[2,4,64,64]{3,2,1,0:T(8,128)S(1)}, s32[]{:T(128)}, bf16[4,2,4]{2,1,0:T(2,128)(2,1)}, /*index=5*/bf16[4,2,...) while((s32[]{:T(128)}, f32[2,4]{1,0:T(2,128)}, f32[2,4,64,64]{3,2,1,0:T(8,128)S(1)}, ...), condition=%wide.region_12.13_spmd, body=%wide.region_11.12_spmd.sunk | while | flops 98326 | bytes 327979 | solution.py:36
  207.5 1.2 convert_exponential_fusion.5
  208.7 1.0 convert_add_fusion.7
  209.7 1.3 convert_exponential_fusion.5
  211.0 1.0 convert_add_fusion.7
  212.0 1.3 convert_exponential_fusion.5
  213.3 1.0 convert_add_fusion.7
  214.5 1.3 exp.143
  215.8 1.5 copy.180
  217.2 1.6 convolution_bitcast_fusion.6
  218.9 1.6 copy.181
  220.5 1.1 fusion.11
  221.6 1.7 fusion.15
  223.3 1.1 fusion.10
  224.4 1.1 fusion.6
  225.5 1.8 rev.23
  227.3 1.6 convolution_bitcast_fusion.7
  229.0 1.7 copy.168
  230.6 1.1 fusion.13
  231.7 1.7 fusion.16
  233.5 1.0 fusion.12
  235.9 1.1 copy.199
  237.0 6.8 %all_to_all.15 = bf16[2,64,512]{2,1,0:T(8,128)(2,1)S(1)} all-to-all(bf16[2,64,512]{2,1,0:T(8,128)(2,1)S(1)} %copy.199), channel_id=1, replica_groups=mesh['sp'=4,'tp'=2,'dp'=4] {'tp'}, dimensions={0} | all-to-all | bytes 262144 | tf_op jit(solution)/shard_map/all_to_all | solution.py:281
  244.1 3.8 %fusion.1 = bf16[64,2048]{1,0:T(8,128)(2,1)} fusion(bf16[64,1024]{1,0:T(8,128)(2,1)S(1)} %bitcast.213, bf16[1024,2048]{1,0:T(8,128)(2,1)} %param.39, bf16[64,2048]{1,0:T(8,128)(2,1)S(1)} %copy-done.7, f32[2048]{0:T(1024)S(1)} %bitcast.239), kind=kOutput, calls=%fused_computation.10 | convolution fusion | flops 268959744 | bytes 4857856 | tf_op jit(solution)/shard_map/dot_general | solution.py:280
  (198 shorter events, 35.8 us)
Async XLA Ops:
  0.0 1.9 copy-start
  1.9 40.6 %copy-start.48 = (bf16[2048]{0:T(1024)(128)(2,1)S(1)}, bf16[2048]{0:T(1024)(128)(2,1)}, u32[]{:S(2)}) copy-start(bf16[2048]{0:T(1024)(128)(2,1)} %param.27) | copy-start | bytes 12292
  1.9 40.6 %copy-start.6 = (bf16[64,2048]{1,0:T(8,128)(2,1)S(1)}, bf16[64,2048]{1,0:T(8,128)(2,1)}, u32[]{:S(2)}) copy-start(bf16[64,2048]{1,0:T(8,128)(2,1)} %param.22) | copy-start | bytes 786436
  42.8 9.4 %copy-start.11 = (bf16[2048,128]{1,0:T(8,128)(2,1)S(1)}, bf16[2048,128]{1,0:T(8,128)(2,1)}, u32[]{:S(2)}) copy-start(bf16[2048,128]{1,0:T(8,128)(2,1)} %param.31) | copy-start | bytes 1572868
  50.0 7.0 %copy-start.2 = (bf16[128,2048]{1,0:T(8,128)(2,1)}, bf16[128,2048]{1,0:T(8,128)(2,1)S(1)}, u32[]{:S(2)}) copy-start(bf16[128,2048]{1,0:T(8,128)(2,1)S(1)} %all_gather.26) | copy-start | bytes 1572868
  50.0 2.6 %copy-start.12 = (bf16[2048,128]{1,0:T(8,128)(2,1)S(1)}, bf16[2048,128]{1,0:T(8,128)(2,1)}, u32[]{:S(2)}) copy-start(bf16[2048,128]{1,0:T(8,128)(2,1)} %param.30) | copy-start | bytes 1572868
  52.3 4.4 %copy-start.27 = (bf16[2,2048,8]{1,2,0:T(8,128)(2,1)S(1)}, bf16[2,2048,8]{1,2,0:T(8,128)(2,1)}, u32[]{:S(2)}) copy-start(bf16[2,2048,8]{1,2,0:T(8,128)(2,1)} %param.32) | copy-start | bytes 196612
  52.3 4.9 %copy-start.54 = (f32[2,8]{1,0:T(2,128)S(1)}, f32[2,8]{1,0:T(2,128)}, u32[]{:S(2)}) copy-start(f32[2,8]{1,0:T(2,128)} %param.36) | copy-start | bytes 196
  52.3 5.0 %copy-start.52 = (f32[128,8]{0,1:T(8,128)S(1)}, f32[128,8]{0,1:T(8,128)}, u32[]{:S(2)}) copy-start(f32[128,8]{0,1:T(8,128)} %param.37) | copy-start | bytes 12292
  52.6 5.3 %copy-start.18 = (bf16[128,128]{1,0:T(8,128)(2,1)}, bf16[128,128]{1,0:T(8,128)(2,1)S(1)}, u32[]{:S(2)}) copy-start(bf16[128,128]{1,0:T(8,128)(2,1)S(1)} %convolution_convert_fusion.4) | copy-start | bytes 98308
  52.9 5.0 %copy-start.19 = (bf16[128,128]{1,0:T(8,128)(2,1)}, bf16[128,128]{1,0:T(8,128)(2,1)S(1)}, u32[]{:S(2)}) copy-start(bf16[128,128]{1,0:T(8,128)(2,1)S(1)} %convolution_convert_fusion.5) | copy-start | bytes 98308
  53.6 105.8 %collective-permute-start = (bf16[2,768]{1,0:T(2,128)(2,1)}, bf16[2,768]{1,0:T(2,128)(2,1)}, u32[]{:S(2)}, u32[]{:S(2)}) collective-permute-start(bf16[2,768]{1,0:T(2,128)(2,1)} %get-tuple-element.220), channel_id=1, source_target_pairs={{0,8},{8,16},{16,24},{1,9},{9,17},{17,25},{2,10},{10,18},{18,26},{... | collective-permute-start | bytes 9224 | tf_op jit(solution)/shard_map/ppermute | solution.py:44
  55.4 103.9 %collective-permute-start.1 = (bf16[2,768]{1,0:T(2,128)(2,1)}, bf16[2,768]{1,0:T(2,128)(2,1)}, u32[]{:S(2)}, u32[]{:S(2)}) collective-permute-start(bf16[2,768]{1,0:T(2,128)(2,1)} %get-tuple-element.221), channel_id=1, source_target_pairs={{8,0},{16,8},{24,16},{9,1},{17,9},{25,17},{10,2},{18,10},{26,18},{... | collective-permute-start | bytes 9224 | tf_op jit(solution)/shard_map/ppermute | solution.py:47
  57.0 29.6 %copy-start.25 = (f32[128,8]{0,1:T(8,128)}, f32[128,8]{0,1:T(8,128)S(1)}, u32[]{:S(2)}) copy-start(f32[128,8]{0,1:T(8,128)S(1)} %compare_select_fusion.3) | copy-start | bytes 12292
  57.3 0.7 copy-start.36
  60.6 2.9 %copy-start.10 = (bf16[128,2048]{1,0:T(8,128)(2,1)S(1)}, bf16[128,2048]{1,0:T(8,128)(2,1)}, u32[]{:S(2)}) copy-start(bf16[128,2048]{1,0:T(8,128)(2,1)} %param.24) | copy-start | bytes 1572868
  60.6 2.9 %copy-start.13 = (bf16[2048,128]{1,0:T(8,128)(2,1)S(1)}, bf16[2048,128]{1,0:T(8,128)(2,1)}, u32[]{:S(2)}) copy-start(bf16[2048,128]{1,0:T(8,128)(2,1)} %param.30) | copy-start | bytes 1572868
  60.7 2.9 %copy-start.45 = (f32[1,2048]{1,0:T(1,128)S(1)}, f32[1,2048]{1,0:T(1,128)}, u32[]{:S(2)}) copy-start(f32[1,2048]{1,0:T(1,128)} %get-tuple-element.227) | copy-start | bytes 24580
  60.7 2.9 %copy-start.46 = (f32[1,2048]{1,0:T(1,128)S(1)}, f32[1,2048]{1,0:T(1,128)}, u32[]{:S(2)}) copy-start(f32[1,2048]{1,0:T(1,128)} %get-tuple-element.228) | copy-start | bytes 24580
  63.6 0.8 copy-start.28
  64.8 14.9 %copy-start.37 = (f32[2,8]{1,0:T(2,128)S(1)}, f32[2,8]{1,0:T(2,128)}, u32[]{:S(2)}) copy-start(f32[2,8]{1,0:T(2,128)} %copy-done.36) | copy-start | bytes 196
  65.2 17.6 %copy-start.41 = (f32[128,8]{0,1:T(8,128)S(1)}, f32[128,8]{0,1:T(8,128)}, u32[]{:S(2)}) copy-start(f32[128,8]{0,1:T(8,128)} %get-tuple-element.233) | copy-start | bytes 12292
  65.2 24.9 %copy-start.38 = (f32[128,8]{0,1:T(8,128)S(1)}, f32[128,8]{0,1:T(8,128)}, u32[]{:S(2)}) copy-start(f32[128,8]{0,1:T(8,128)} %get-tuple-element.232) | copy-start | bytes 12292
  79.7 1.5 copy-start.5
  100.9 5.5 %copy-start.39 = (f32[128,8]{0,1:T(8,128)S(1)}, f32[128,8]{0,1:T(8,128)}, u32[]{:S(2)}) copy-start(f32[128,8]{0,1:T(8,128)} %rev.22) | copy-start | bytes 12292
  101.8 0.6 copy-start.21
  110.2 3.2 %copy-start.22 = (f32[2,512,8]{1,2,0:T(8,128)S(1)}, f32[2,512,8]{1,2,0:T(8,128)}, u32[]{:S(2)}) copy-start(f32[2,512,8]{1,2,0:T(8,128)} %copy-done.21) | copy-start | bytes 98308
  110.2 3.2 %copy-start.24 = (f32[2,512,8]{1,2,0:T(8,128)S(1)}, f32[2,512,8]{1,2,0:T(8,128)}, u32[]{:S(2)}) copy-start(f32[2,512,8]{1,2,0:T(8,128)} %maximum_multiply_fusion) | copy-start | bytes 98308
  110.2 3.2 %copy-start.53 = (f32[8]{0:T(128)S(1)}, f32[8]{0:T(128)}, u32[]{:S(2)}) copy-start(f32[8]{0:T(128)} %slice_reduce_fusion.1) | copy-start | bytes 100
  110.2 4.6 %copy-start.50 = (f32[2,4]{1,0:T(2,128)S(1)}, f32[2,4]{1,0:T(2,128)}, u32[]{:S(2)}) copy-start(f32[2,4]{1,0:T(2,128)} %slice_bitcast_fusion.3) | copy-start | bytes 100
  110.2 4.6 %copy-start.15 = (f32[128,2,4]{2,1,0:T(2,128)S(1)}, f32[128,2,4]{2,1,0:T(2,128)}, u32[]{:S(2)}) copy-start(f32[128,2,4]{2,1,0:T(2,128)} %copy.175) | copy-start | bytes 12292
  110.2 5.3 %copy-start.51 = (f32[2,4]{1,0:T(2,128)S(1)}, f32[2,4]{1,0:T(2,128)}, u32[]{:S(2)}) copy-start(f32[2,4]{1,0:T(2,128)} %slice_bitcast_fusion.2) | copy-start | bytes 100
  110.2 5.3 %copy-start.16 = (f32[128,2,4]{2,1,0:T(2,128)S(1)}, f32[128,2,4]{2,1,0:T(2,128)}, u32[]{:S(2)}) copy-start(f32[128,2,4]{2,1,0:T(2,128)} %copy.188) | copy-start | bytes 12292
  110.2 6.1 %copy-start.1 = (f32[515,640]{0,1:T(8,128)S(1)}, f32[515,640]{0,1:T(8,128)}, u32[]{:S(2)}) copy-start(f32[515,640]{0,1:T(8,128)} %pad_convert_fusion) | copy-start | bytes 3955204
  110.2 6.1 %copy-start.42 = (f32[640]{0:T(1024)S(1)}, f32[640]{0:T(1024)}, u32[]{:S(2)}) copy-start(f32[640]{0:T(1024)} %get-tuple-element.183) | copy-start | bytes 7684
  110.2 6.1 %copy-start.43 = (f32[640]{0:T(1024)S(1)}, f32[640]{0:T(1024)}, u32[]{:S(2)}) copy-start(f32[640]{0:T(1024)} %get-tuple-element.184) | copy-start | bytes 7684
  110.2 6.1 %copy-start.44 = (f32[640]{0:T(1024)S(1)}, f32[640]{0:T(1024)}, u32[]{:S(2)}) copy-start(f32[640]{0:T(1024)} %get-tuple-element.185) | copy-start | bytes 7684
  116.3 2.4 copy-start.55
  116.3 12.8 %copy-start.56 = (bf16[1,2,4]{2,1,0:T(2,128)(2,1)S(1)}, bf16[1,2,4]{2,1,0:T(2,128)(2,1)}, u32[]{:S(2)}) copy-start(bf16[1,2,4]{2,1,0:T(2,128)(2,1)} %convert_element_type.248) | copy-start | bytes 52
  144.2 16.0 %copy-start.31 = (f32[768]{0:T(1024)S(1)}, f32[768]{0:T(1024)}, u32[]{:S(2)}) copy-start(f32[768]{0:T(1024)} %get-tuple-element.178) | copy-start | bytes 9220
  144.2 16.0 %copy-start.32 = (f32[768]{0:T(1024)S(1)}, f32[768]{0:T(1024)}, u32[]{:S(2)}) copy-start(f32[768]{0:T(1024)} %get-tuple-element.179) | copy-start | bytes 9220
  144.2 16.0 %copy-start.33 = (f32[768]{0:T(1024)S(1)}, f32[768]{0:T(1024)}, u32[]{:S(2)}) copy-start(f32[768]{0:T(1024)} %get-tuple-element.180) | copy-start | bytes 9220
  144.2 16.0 %copy-start.34 = (f32[768]{0:T(1024)S(1)}, f32[768]{0:T(1024)}, u32[]{:S(2)}) copy-start(f32[768]{0:T(1024)} %get-tuple-element.181) | copy-start | bytes 9220
  160.2 3.9 %copy-start.47 = (f32[2,4]{1,0:T(2,128)S(1)}, f32[2,4]{1,0:T(2,128)}, u32[]{:S(2)}) copy-start(f32[2,4]{1,0:T(2,128)} %exponential_multiply_fusion.3) | copy-start | bytes 100
  162.1 18.8 %copy-start.20 = (bf16[128,128]{0,1:T(8,128)(2,1)}, bf16[128,128]{0,1:T(8,128)(2,1)S(1)}, u32[]{:S(2)}) copy-start(bf16[128,128]{0,1:T(8,128)(2,1)S(1)} %copy.166) | copy-start | bytes 98308
  181.5 25.4 %copy-start.3 = (f32[2,4,64,64]{3,2,1,0:T(8,128)}, f32[2,4,64,64]{3,2,1,0:T(8,128)S(1)}, u32[]{:S(2)}) copy-start(f32[2,4,64,64]{3,2,1,0:T(8,128)S(1)} %get-tuple-element.175) | copy-start | bytes 393220
  220.5 3.9 %copy-start.14 = (bf16[128,512]{0,1:T(8,128)(2,1)S(1)}, bf16[128,512]{0,1:T(8,128)(2,1)}, u32[]{:S(2)}) copy-start(bf16[128,512]{0,1:T(8,128)(2,1)} %copy.178) | copy-start | bytes 393220
  220.5 3.9 %copy-start.23 = (f32[128,128,2]{1,0,2:T(8,128)S(1)}, f32[128,128,2]{1,0,2:T(8,128)}, u32[]{:S(2)}) copy-start(f32[128,128,2]{1,0,2:T(8,128)} %copy.181) | copy-start | bytes 393220
  220.5 3.9 %copy-start.40 = (f32[128,8]{0,1:T(8,128)S(1)}, f32[128,8]{0,1:T(8,128)}, u32[]{:S(2)}) copy-start(f32[128,8]{0,1:T(8,128)} %rev.22) | copy-start | bytes 12292
  220.5 3.9 %copy-start.49 = (f32[128,2,4]{0,2,1:T(4,128)S(1)}, f32[128,2,4]{0,2,1:T(4,128)}, u32[]{:S(2)}) copy-start(f32[128,2,4]{0,2,1:T(4,128)} %copy.183) | copy-start | bytes 12292
  223.3 8.4 %copy-start.4 = (f32[2,4,64,64]{3,2,1,0:T(8,128)S(1)}, f32[2,4,64,64]{3,2,1,0:T(8,128)}, u32[]{:S(2)}) copy-start(f32[2,4,64,64]{3,2,1,0:T(8,128)} %copy-done.3) | copy-start | bytes 393220
  230.6 3.9 %copy-start.8 = (f32[128,512]{0,1:T(8,128)S(1)}, f32[128,512]{0,1:T(8,128)}, u32[]{:S(2)}) copy-start(f32[128,512]{0,1:T(8,128)} %copy.190) | copy-start | bytes 786436
  230.6 3.9 %copy-start.9 = (f32[128,2,4,64]{0,3,2,1:T(8,128)S(1)}, f32[128,2,4,64]{0,3,2,1:T(8,128)}, u32[]{:S(2)}) copy-start(f32[128,2,4,64]{0,3,2,1:T(8,128)} %rev.23) | copy-start | bytes 786436
  230.6 3.9 %copy-start.17 = (f32[128,128,2]{1,0,2:T(8,128)S(1)}, f32[128,128,2]{1,0,2:T(8,128)}, u32[]{:S(2)}) copy-start(f32[128,128,2]{1,0,2:T(8,128)} %copy.168) | copy-start | bytes 393220
  230.6 3.9 %copy-start.26 = (f32[128,8]{0,1:T(8,128)S(1)}, f32[128,8]{0,1:T(8,128)}, u32[]{:S(2)}) copy-start(f32[128,8]{0,1:T(8,128)} %copy-done.25) | copy-start | bytes 12292
  230.6 3.9 %copy-start.29 = (f32[128,2,4]{0,2,1:T(4,128)S(1)}, f32[128,2,4]{0,2,1:T(4,128)}, u32[]{:S(2)}) copy-start(f32[128,2,4]{0,2,1:T(4,128)} %copy.170) | copy-start | bytes 12292
  231.7 3.2 %copy-start.35 = (f32[2,4,64]{2,1,0:T(4,128)S(1)}, f32[2,4,64]{2,1,0:T(4,128)}, u32[]{:S(2)}) copy-start(f32[2,4,64]{2,1,0:T(4,128)} %reshape.218) | copy-start | bytes 6148
  234.5 9.5 %copy-start.7 = (bf16[64,2048]{1,0:T(8,128)(2,1)S(1)}, bf16[64,2048]{1,0:T(8,128)(2,1)}, u32[]{:S(2)}) copy-start(bf16[64,2048]{1,0:T(8,128)(2,1)} %param.22) | copy-start | bytes 786436
  234.9 9.1 %copy-start.30 = (f32[1,2048]{1,0:T(1,128)S(1)}, f32[1,2048]{1,0:T(1,128)}, u32[]{:S(2)}) copy-start(f32[1,2048]{1,0:T(1,128)} %get-tuple-element.226) | copy-start | bytes 24580
where the time goes:
time: 250 us; the launch traced here: 248 us
  blocking collectives  122 us (49%)
  local copies, waits for them, and re-layouts  58.6 us (23%)
  other arithmetic  34.5 us (14%)
  matrix products  28.4 us (11%)
  starting transfers between devices  3.15 us (1%)
    all_gather x4, blocking collectives, prefix(): lax.all_gather(a.astype(kind), axis)  54.2 us
    psum x1, blocking collectives, local(): lax.psum(jnp.dot(own_cols, modulation, preferred_element_type=jnp.float32...  39.4 us
    all_gather x1, blocking collectives, local(): context_cols = lax.all_gather(own_context, 'sp', axis=0, tiled=True)  14.5 us
    dot_general x10, matrix products, project_many(): jnp.dot(row_block, weight, preferred_element_type=jnp.float32)  10.5 us
    all_gather x1, blocking collectives, local(): lax.all_gather(hidden, 'tp', axis=0, tiled=True)  7.17 us
    all_to_all x1, blocking collectives, local(): lax.all_to_all(stacked, 'tp', split_axis=0, concat_axis=2, tiled=True)[0]  6.85 us
    another operation x3, other arithmetic  6.56 us
    exp x4, local copies, waits for them, and re-layouts, directed_pass(): jnp.exp(running)  5.96 us
  transfers between devices with their start and end apart: 2, of which 0 were waited for; matrix products, arithmetic and copies ran while one was open for 28% of the time, Pallas kernels for 0%

commit v1 on v0

--- a/solution.py
+++ b/solution.py
@@ -9,6 +9,12 @@
 ROW_EPS = 1e-06
 GROUP_EPS = 1e-05
 HIGHEST = lax.Precision.HIGHEST
+
+
+def plan_region(piece_in):
+    for c in ("tp", "sp"):
+        piece_in = lax.psum(piece_in, axis_name=c)
+    return piece_in
 
 
 def prefix(x, axis, join, neutral, backward):
@@ -206,9 +212,7 @@
     own_cols = lax.dynamic_slice_in_dim(
         cond_rows, lax.axis_index(("sp", "tp")) * mod_share, mod_share, 1
     )
-    mod_rows = lax.psum(
-        jnp.dot(own_cols, modulation, preferred_element_type=jnp.float32), ("sp", "tp")
-    )
+    mod_rows = plan_region(jnp.dot(own_cols, modulation, preferred_element_type=jnp.float32))
     shift_rows = mod_rows[:, :model_width]
     scale_rows = mod_rows[:, model_width : 2 * model_width]
     gate_row = mod_rows[0, 2 * model_width :]

time: 250 us -> 241 us (0.964)
  blocking collectives: 122 us -> 112 us
    psum x1 -> x2, blocking collectives: 39.4 us -> 29.7 us  [plan_region(): piece_in = lax.psum(piece_in, axis_name=c)]
  transfers between devices with their start and end apart: 2 -> 2, of which waited for: 0 -> 0; matrix products, arithmetic and copies ran while one was open for 28% -> 29% of each run, Pallas kernels for 0% -> 0%
where the time goes in v1:
time: 241 us; the launch traced here: 238 us
  blocking collectives  112 us (46%)
  local copies, waits for them, and re-layouts  58.5 us (24%)
  other arithmetic  34.5 us (14%)
  matrix products  28.4 us (12%)
  starting transfers between devices  3.13 us (1%)
    all_gather x4, blocking collectives, prefix(): lax.all_gather(a.astype(kind), axis)  53.3 us
    psum x2, blocking collectives, plan_region(): piece_in = lax.psum(piece_in, axis_name=c)  29.7 us
    all_gather x1, blocking collectives, local(): context_cols = lax.all_gather(own_context, 'sp', axis=0, tiled=True)  15.4 us
    dot_general x10, matrix products, project_many(): jnp.dot(row_block, weight, preferred_element_type=jnp.float32)  10.5 us
    all_gather x1, blocking collectives, local(): lax.all_gather(hidden, 'tp', axis=0, tiled=True)  7.17 us
    all_to_all x1, blocking collectives, local(): lax.all_to_all(stacked, 'tp', split_axis=0, concat_axis=2, tiled=True)[0]  6.85 us
    another operation x3, other arithmetic  6.54 us
    exp x4, local copies, waits for them, and re-layouts, directed_pass(): jnp.exp(running)  5.94 us
  transfers between devices with their start and end apart: 2, of which 0 were waited for; matrix products, arithmetic and copies ran while one was open for 29% of the time, Pallas kernels for 0%

profile of v1, /device:TPU:0, one launch (start us, length us, event | category | flops | bytes accessed | tf_op | source)
XLA Modules:
  0.0 238.1 jit_solution(14406622085925360747)
XLA Ops:
  2.4 10.3 %psum.14 = f32[2,6144]{1,0:T(2,128)S(1)} all-reduce(f32[2,6144]{1,0:T(2,128)S(1)} %fusion.93), channel_id=1, replica_groups=mesh['sp'=4,'tp'=2,'dp'=4] {'tp'}, use_global_device_ids=true, to_apply=%region_0.1 | all-reduce | flops 12288 | bytes 98304 | tf_op jit(solution)/shard_map/psum | solution.py:16
  12.7 19.5 %psum.15 = f32[2,6144]{1,0:T(2,128)S(1)} all-reduce(f32[2,6144]{1,0:T(2,128)S(1)} %psum.14), channel_id=1, replica_groups=mesh['sp'=4,'tp'=2,'dp'=4] {'sp'}, use_global_device_ids=true, to_apply=%region_1.2 | all-reduce | flops 12288 | bytes 98304 | tf_op jit(solution)/shard_map/psum | solution.py:16
  33.2 7.2 %all_gather.26 = bf16[128,2048]{1,0:T(8,128)(2,1)S(1)} all-gather(bf16[64,2048]{1,0:T(8,128)(2,1)S(1)} %fusion.31), channel_id=1, replica_groups=mesh['sp'=4,'tp'=2,'dp'=4] {'tp'}, dimensions={0}, use_global_device_ids=true | all-gather | bytes 786432 | tf_op jit(solution)/shard_map/all_gather | solution.py:226
  40.4 2.3 convolution_convert_fusion.2
  43.9 1.9 collective-permute-start
  45.8 1.3 collective-permute-start.1
  49.8 1.2 fusion.22
  51.0 2.9 %convolution_convert_fusion.1 = bf16[128,512]{0,1:T(8,128)(2,1)S(1)} fusion(bf16[2048,512]{1,0:T(8,128)(2,1)} %param.28, bf16[128,2048]{1,0:T(8,128)(2,1)} %param.24, f32[2048]{0:T(1024)} %bitcast.249, f32[2048]{0:T(1024)} %bitcast.253, f32[2048]{0:T(1024)S(1)} %convert_element_type.221, f32[128]{0:T(128)S(1)} %add_rsqrt_fusion.1), kind=kOutput, calls=%fused_computation.49 | convolution fusion | flops 270073856 | bytes 2777600 | tf_op jit(solution)/shard_map/dot_general | solution.py:69
  55.6 15.4 %all_gather.30 = bf16[512,656]{0,1:T(8,128)(2,1)S(1)} all-gather(bf16[128,656]{0,1:T(8,128)(2,1)S(1)} %pad_maximum_fusion), channel_id=1, replica_groups=mesh['sp'=4,'tp'=2,'dp'=4] {'sp'}, dimensions={0}, use_global_device_ids=true | all-gather | bytes 839680 | tf_op jit(solution)/shard_map/all_gather | solution.py:247
  74.9 1.0 fusion.114
  82.0 1.6 reduce_window_sum.52
  84.9 5.0 %reduce-window.6 = f32[2,8,4,128]{3,1,2,0:T(8,128)} reduce-window(f32[2,8,4,128]{3,1,2,0:T(8,128)} %fusion.148, f32[]{:T(128)} %constant.128.clone.1), window={size=1x1x1x128 pad=0_0x0_0x0_0x127_0}, to_apply=%region_8.9 | reduce-window | flops 1040384 | bytes 65540 | tf_op jit(solution)/shard_map/reduce-window
  89.9 1.5 slice_reduce_fusion
  94.4 2.7 %pad_convert_fusion = f32[515,640]{0,1:T(8,128)} fusion(bf16[512,640]{0,1:T(8,128)(2,1)} %slice.222), kind=kLoop, calls=%fused_computation.67 | loop fusion | flops 329600 | bytes 1973760 | tf_op jit(solution)/shard_map/convert_element_type | solution.py:77
  98.4 1.6 reduce_window_sum.56
  101.4 3.1 %divide_multiply_fusion = f32[128,512]{1,0:T(8,128)} fusion(bf16[128,2048]{1,0:T(8,128)(2,1)} %copy-done.2, bf16[2048,512]{1,0:T(8,128)(2,1)} %param.29), kind=kOutput, calls=%fused_computation.89 | convolution fusion | flops 268828672 | bytes 2883584 | tf_op jit(solution)/shard_map/dot_general | solution.py:69
  104.5 1.4 fusion.76
  107.5 2.4 multiply_convert_fusion
  109.9 9.0 %all_gather.27 = bf16[4,2,4]{2,1,0:T(2,128)(2,1)} all-gather(bf16[1,2,4]{2,1,0:T(2,128)(2,1)S(1)} %copy-done.55), channel_id=1, replica_groups=mesh['sp'=4,'tp'=2,'dp'=4] {'sp'}, dimensions={0}, use_global_device_ids=true | all-gather | bytes 80 | tf_op jit(solution)/shard_map/all_gather | solution.py:25
  118.9 8.4 %all_gather.31 = bf16[4,2,4]{2,1,0:T(2,128)(2,1)} all-gather(bf16[1,2,4]{2,1,0:T(2,128)(2,1)S(1)} %copy-done.56), channel_id=1, replica_groups=mesh['sp'=4,'tp'=2,'dp'=4] {'sp'}, dimensions={0}, use_global_device_ids=true | all-gather | bytes 80 | tf_op jit(solution)/shard_map/all_gather | solution.py:25
  127.2 1.9 slice.230
  129.1 1.6 slice.231
  130.7 1.5 exp.128
  132.1 1.5 exp.139
  135.9 1.3 reshape.201
  137.3 1.5 copy.174
  138.8 1.3 reshape.203
  140.1 1.6 copy.189
  141.7 1.5 copy.187
  143.2 1.6 copy.185
  144.8 1.6 copy.172
  146.3 1.8 copy.190
  148.1 1.3 reshape.218
  150.8 1.3 rev.18
  154.4 15.4 %all-gather = bf16[8,4,64,64]{3,2,1,0:T(8,128)(2,1)} all-gather(bf16[2,4,64,64]{3,2,1,0:T(8,128)(2,1)S(1)} %fusion.17), channel_id=2, replica_groups=mesh['sp'=4,'tp'=2,'dp'=4] {'sp'}, dimensions={0}, use_global_device_ids=true | all-gather | bytes 327680 | tf_op jit(solution)/shard_map/all_gather | solution.py:25
  170.4 1.2 exp.132
  171.6 1.6 copy.178
  173.3 1.5 copy.179
  175.5 1.1 fusion.18
  176.6 20.6 %all-gather.1 = bf16[8,4,64,64]{3,2,1,0:T(8,128)(2,1)} all-gather(bf16[2,4,64,64]{3,2,1,0:T(8,128)(2,1)S(1)} %fusion.18), channel_id=3, replica_groups=mesh['sp'=4,'tp'=2,'dp'=4] {'sp'}, dimensions={0}, use_global_device_ids=true | all-gather | bytes 327680 | tf_op jit(solution)/shard_map/all_gather | solution.py:25
  197.8 7.0 %while.7 = (s32[]{:T(128)}, f32[2,4]{1,0:T(2,128)}, f32[2,4,64,64]{3,2,1,0:T(8,128)S(1)}, s32[]{:T(128)}, bf16[4,2,4]{2,1,0:T(2,128)(2,1)}, /*index=5*/bf16[4,2,...) while((s32[]{:T(128)}, f32[2,4]{1,0:T(2,128)}, f32[2,4,64,64]{3,2,1,0:T(8,128)S(1)}, ...), condition=%wide.region_13.14_spmd, body=%wide.region_12.13_spmd.sunk | while | flops 98326 | bytes 327979 | solution.py:42
  197.8 1.2 convert_exponential_fusion.5
  199.0 1.0 convert_add_fusion.7
  200.1 1.3 convert_exponential_fusion.5
  201.3 1.0 convert_add_fusion.7
  202.4 1.3 convert_exponential_fusion.5
  203.6 1.0 convert_add_fusion.7
  204.8 1.3 exp.143
  206.1 1.5 copy.180
  207.6 1.6 convolution_bitcast_fusion.6
  209.2 1.7 copy.181
  210.9 1.0 fusion.11
  211.9 1.7 fusion.15
  213.7 1.1 fusion.10
  214.8 1.1 fusion.6
  215.8 1.8 rev.23
  217.6 1.6 convolution_bitcast_fusion.7
  219.3 1.7 copy.168
  221.0 1.1 fusion.13
  222.0 1.7 fusion.16
  223.8 1.0 fusion.12
  226.3 1.1 copy.199
  227.3 6.8 %all_to_all.15 = bf16[2,64,512]{2,1,0:T(8,128)(2,1)S(1)} all-to-all(bf16[2,64,512]{2,1,0:T(8,128)(2,1)S(1)} %copy.199), channel_id=1, replica_groups=mesh['sp'=4,'tp'=2,'dp'=4] {'tp'}, dimensions={0} | all-to-all | bytes 262144 | tf_op jit(solution)/shard_map/all_to_all | solution.py:285
  234.4 3.8 %fusion.1 = bf16[64,2048]{1,0:T(8,128)(2,1)} fusion(bf16[64,1024]{1,0:T(8,128)(2,1)S(1)} %bitcast.213, bf16[1024,2048]{1,0:T(8,128)(2,1)} %param.39, bf16[64,2048]{1,0:T(8,128)(2,1)S(1)} %copy-done.7, f32[2048]{0:T(1024)S(1)} %bitcast.239), kind=kOutput, calls=%fused_computation.10 | convolution fusion | flops 268959744 | bytes 4857856 | tf_op jit(solution)/shard_map/dot_general | solution.py:284
  (199 shorter events, 36.8 us)
Async XLA Ops:
  0.0 1.9 copy-start
  1.9 30.9 %copy-start.48 = (bf16[2048]{0:T(1024)(128)(2,1)S(1)}, bf16[2048]{0:T(1024)(128)(2,1)}, u32[]{:S(2)}) copy-start(bf16[2048]{0:T(1024)(128)(2,1)} %param.27) | copy-start | bytes 12292
  1.9 30.9 %copy-start.6 = (bf16[64,2048]{1,0:T(8,128)(2,1)S(1)}, bf16[64,2048]{1,0:T(8,128)(2,1)}, u32[]{:S(2)}) copy-start(bf16[64,2048]{1,0:T(8,128)(2,1)} %param.22) | copy-start | bytes 786436
  33.2 9.5 %copy-start.11 = (bf16[2048,128]{1,0:T(8,128)(2,1)S(1)}, bf16[2048,128]{1,0:T(8,128)(2,1)}, u32[]{:S(2)}) copy-start(bf16[2048,128]{1,0:T(8,128)(2,1)} %param.31) | copy-start | bytes 1572868
  40.4 6.9 %copy-start.2 = (bf16[128,2048]{1,0:T(8,128)(2,1)}, bf16[128,2048]{1,0:T(8,128)(2,1)S(1)}, u32[]{:S(2)}) copy-start(bf16[128,2048]{1,0:T(8,128)(2,1)S(1)} %all_gather.26) | copy-start | bytes 1572868
  40.4 2.6 %copy-start.12 = (bf16[2048,128]{1,0:T(8,128)(2,1)S(1)}, bf16[2048,128]{1,0:T(8,128)(2,1)}, u32[]{:S(2)}) copy-start(bf16[2048,128]{1,0:T(8,128)(2,1)} %param.30) | copy-start | bytes 1572868
  42.6 4.4 %copy-start.27 = (bf16[2,2048,8]{1,2,0:T(8,128)(2,1)S(1)}, bf16[2,2048,8]{1,2,0:T(8,128)(2,1)}, u32[]{:S(2)}) copy-start(bf16[2,2048,8]{1,2,0:T(8,128)(2,1)} %param.32) | copy-start | bytes 196612
  42.6 4.9 %copy-start.54 = (f32[2,8]{1,0:T(2,128)S(1)}, f32[2,8]{1,0:T(2,128)}, u32[]{:S(2)}) copy-start(f32[2,8]{1,0:T(2,128)} %param.36) | copy-start | bytes 196
  42.7 5.0 %copy-start.52 = (f32[128,8]{0,1:T(8,128)S(1)}, f32[128,8]{0,1:T(8,128)}, u32[]{:S(2)}) copy-start(f32[128,8]{0,1:T(8,128)} %param.37) | copy-start | bytes 12292
  43.0 5.3 %copy-start.18 = (bf16[128,128]{1,0:T(8,128)(2,1)}, bf16[128,128]{1,0:T(8,128)(2,1)S(1)}, u32[]{:S(2)}) copy-start(bf16[128,128]{1,0:T(8,128)(2,1)S(1)} %convolution_convert_fusion.4) | copy-start | bytes 98308
  43.3 5.0 %copy-start.19 = (bf16[128,128]{1,0:T(8,128)(2,1)}, bf16[128,128]{1,0:T(8,128)(2,1)S(1)}, u32[]{:S(2)}) copy-start(bf16[128,128]{1,0:T(8,128)(2,1)S(1)} %convolution_convert_fusion.5) | copy-start | bytes 98308
  43.9 105.6 %collective-permute-start = (bf16[2,768]{1,0:T(2,128)(2,1)}, bf16[2,768]{1,0:T(2,128)(2,1)}, u32[]{:S(2)}, u32[]{:S(2)}) collective-permute-start(bf16[2,768]{1,0:T(2,128)(2,1)} %get-tuple-element.220), channel_id=1, source_target_pairs={{0,8},{8,16},{16,24},{1,9},{9,17},{17,25},{2,10},{10,18},{18,26},{... | collective-permute-start | bytes 9224 | tf_op jit(solution)/shard_map/ppermute | solution.py:50
  45.8 103.7 %collective-permute-start.1 = (bf16[2,768]{1,0:T(2,128)(2,1)}, bf16[2,768]{1,0:T(2,128)(2,1)}, u32[]{:S(2)}, u32[]{:S(2)}) collective-permute-start(bf16[2,768]{1,0:T(2,128)(2,1)} %get-tuple-element.221), channel_id=1, source_target_pairs={{8,0},{16,8},{24,16},{9,1},{17,9},{25,17},{10,2},{18,10},{26,18},{... | collective-permute-start | bytes 9224 | tf_op jit(solution)/shard_map/ppermute | solution.py:53
  47.3 30.5 %copy-start.25 = (f32[128,8]{0,1:T(8,128)}, f32[128,8]{0,1:T(8,128)S(1)}, u32[]{:S(2)}) copy-start(f32[128,8]{0,1:T(8,128)S(1)} %compare_select_fusion.3) | copy-start | bytes 12292
  47.6 0.7 copy-start.36
  51.0 2.9 %copy-start.10 = (bf16[128,2048]{1,0:T(8,128)(2,1)S(1)}, bf16[128,2048]{1,0:T(8,128)(2,1)}, u32[]{:S(2)}) copy-start(bf16[128,2048]{1,0:T(8,128)(2,1)} %param.24) | copy-start | bytes 1572868
  51.0 2.9 %copy-start.13 = (bf16[2048,128]{1,0:T(8,128)(2,1)S(1)}, bf16[2048,128]{1,0:T(8,128)(2,1)}, u32[]{:S(2)}) copy-start(bf16[2048,128]{1,0:T(8,128)(2,1)} %param.30) | copy-start | bytes 1572868
  51.0 2.9 %copy-start.45 = (f32[1,2048]{1,0:T(1,128)S(1)}, f32[1,2048]{1,0:T(1,128)}, u32[]{:S(2)}) copy-start(f32[1,2048]{1,0:T(1,128)} %get-tuple-element.227) | copy-start | bytes 24580
  51.0 2.9 %copy-start.46 = (f32[1,2048]{1,0:T(1,128)S(1)}, f32[1,2048]{1,0:T(1,128)}, u32[]{:S(2)}) copy-start(f32[1,2048]{1,0:T(1,128)} %get-tuple-element.228) | copy-start | bytes 24580
  53.9 0.8 copy-start.28
  55.1 15.8 %copy-start.37 = (f32[2,8]{1,0:T(2,128)S(1)}, f32[2,8]{1,0:T(2,128)}, u32[]{:S(2)}) copy-start(f32[2,8]{1,0:T(2,128)} %copy-done.36) | copy-start | bytes 196
  55.5 18.5 %copy-start.41 = (f32[128,8]{0,1:T(8,128)S(1)}, f32[128,8]{0,1:T(8,128)}, u32[]{:S(2)}) copy-start(f32[128,8]{0,1:T(8,128)} %get-tuple-element.233) | copy-start | bytes 12292
  55.5 25.7 %copy-start.38 = (f32[128,8]{0,1:T(8,128)S(1)}, f32[128,8]{0,1:T(8,128)}, u32[]{:S(2)}) copy-start(f32[128,8]{0,1:T(8,128)} %get-tuple-element.232) | copy-start | bytes 12292
  70.9 1.5 copy-start.5
  92.1 5.5 %copy-start.39 = (f32[128,8]{0,1:T(8,128)S(1)}, f32[128,8]{0,1:T(8,128)}, u32[]{:S(2)}) copy-start(f32[128,8]{0,1:T(8,128)} %rev.22) | copy-start | bytes 12292
  93.0 0.6 copy-start.21
  101.3 3.2 %copy-start.22 = (f32[2,512,8]{1,2,0:T(8,128)S(1)}, f32[2,512,8]{1,2,0:T(8,128)}, u32[]{:S(2)}) copy-start(f32[2,512,8]{1,2,0:T(8,128)} %copy-done.21) | copy-start | bytes 98308
  101.4 3.2 %copy-start.24 = (f32[2,512,8]{1,2,0:T(8,128)S(1)}, f32[2,512,8]{1,2,0:T(8,128)}, u32[]{:S(2)}) copy-start(f32[2,512,8]{1,2,0:T(8,128)} %maximum_multiply_fusion) | copy-start | bytes 98308
  101.4 3.2 %copy-start.53 = (f32[8]{0:T(128)S(1)}, f32[8]{0:T(128)}, u32[]{:S(2)}) copy-start(f32[8]{0:T(128)} %slice_reduce_fusion.1) | copy-start | bytes 100
  101.4 4.6 %copy-start.50 = (f32[2,4]{1,0:T(2,128)S(1)}, f32[2,4]{1,0:T(2,128)}, u32[]{:S(2)}) copy-start(f32[2,4]{1,0:T(2,128)} %slice_bitcast_fusion.3) | copy-start | bytes 100
  101.4 4.6 %copy-start.15 = (f32[128,2,4]{2,1,0:T(2,128)S(1)}, f32[128,2,4]{2,1,0:T(2,128)}, u32[]{:S(2)}) copy-start(f32[128,2,4]{2,1,0:T(2,128)} %copy.175) | copy-start | bytes 12292
  101.4 5.3 %copy-start.51 = (f32[2,4]{1,0:T(2,128)S(1)}, f32[2,4]{1,0:T(2,128)}, u32[]{:S(2)}) copy-start(f32[2,4]{1,0:T(2,128)} %slice_bitcast_fusion.2) | copy-start | bytes 100
  101.4 5.3 %copy-start.16 = (f32[128,2,4]{2,1,0:T(2,128)S(1)}, f32[128,2,4]{2,1,0:T(2,128)}, u32[]{:S(2)}) copy-start(f32[128,2,4]{2,1,0:T(2,128)} %copy.188) | copy-start | bytes 12292
  101.4 6.1 %copy-start.1 = (f32[515,640]{0,1:T(8,128)S(1)}, f32[515,640]{0,1:T(8,128)}, u32[]{:S(2)}) copy-start(f32[515,640]{0,1:T(8,128)} %pad_convert_fusion) | copy-start | bytes 3955204
  101.4 6.1 %copy-start.42 = (f32[640]{0:T(1024)S(1)}, f32[640]{0:T(1024)}, u32[]{:S(2)}) copy-start(f32[640]{0:T(1024)} %get-tuple-element.183) | copy-start | bytes 7684
  101.4 6.0 %copy-start.43 = (f32[640]{0:T(1024)S(1)}, f32[640]{0:T(1024)}, u32[]{:S(2)}) copy-start(f32[640]{0:T(1024)} %get-tuple-element.184) | copy-start | bytes 7684
  101.4 6.0 %copy-start.44 = (f32[640]{0:T(1024)S(1)}, f32[640]{0:T(1024)}, u32[]{:S(2)}) copy-start(f32[640]{0:T(1024)} %get-tuple-element.185) | copy-start | bytes 7684
  107.5 2.4 %copy-start.55 = (bf16[1,2,4]{2,1,0:T(2,128)(2,1)S(1)}, bf16[1,2,4]{2,1,0:T(2,128)(2,1)}, u32[]{:S(2)}) copy-start(bf16[1,2,4]{2,1,0:T(2,128)(2,1)} %convert_element_type.233) | copy-start | bytes 52
  107.5 11.4 %copy-start.56 = (bf16[1,2,4]{2,1,0:T(2,128)(2,1)S(1)}, bf16[1,2,4]{2,1,0:T(2,128)(2,1)}, u32[]{:S(2)}) copy-start(bf16[1,2,4]{2,1,0:T(2,128)(2,1)} %convert_element_type.248) | copy-start | bytes 52
  134.3 16.0 %copy-start.31 = (f32[768]{0:T(1024)S(1)}, f32[768]{0:T(1024)}, u32[]{:S(2)}) copy-start(f32[768]{0:T(1024)} %get-tuple-element.178) | copy-start | bytes 9220
  134.3 16.0 %copy-start.32 = (f32[768]{0:T(1024)S(1)}, f32[768]{0:T(1024)}, u32[]{:S(2)}) copy-start(f32[768]{0:T(1024)} %get-tuple-element.179) | copy-start | bytes 9220
  134.3 16.1 %copy-start.33 = (f32[768]{0:T(1024)S(1)}, f32[768]{0:T(1024)}, u32[]{:S(2)}) copy-start(f32[768]{0:T(1024)} %get-tuple-element.180) | copy-start | bytes 9220
  134.3 16.1 %copy-start.34 = (f32[768]{0:T(1024)S(1)}, f32[768]{0:T(1024)}, u32[]{:S(2)}) copy-start(f32[768]{0:T(1024)} %get-tuple-element.181) | copy-start | bytes 9220
  150.3 3.9 %copy-start.47 = (f32[2,4]{1,0:T(2,128)S(1)}, f32[2,4]{1,0:T(2,128)}, u32[]{:S(2)}) copy-start(f32[2,4]{1,0:T(2,128)} %exponential_multiply_fusion.3) | copy-start | bytes 100
  152.2 17.6 %copy-start.20 = (bf16[128,128]{0,1:T(8,128)(2,1)}, bf16[128,128]{0,1:T(8,128)(2,1)S(1)}, u32[]{:S(2)}) copy-start(bf16[128,128]{0,1:T(8,128)(2,1)S(1)} %copy.166) | copy-start | bytes 98308
  170.4 26.8 %copy-start.3 = (f32[2,4,64,64]{3,2,1,0:T(8,128)}, f32[2,4,64,64]{3,2,1,0:T(8,128)S(1)}, u32[]{:S(2)}) copy-start(f32[2,4,64,64]{3,2,1,0:T(8,128)S(1)} %get-tuple-element.175) | copy-start | bytes 393220
  210.9 3.9 %copy-start.14 = (bf16[128,512]{0,1:T(8,128)(2,1)S(1)}, bf16[128,512]{0,1:T(8,128)(2,1)}, u32[]{:S(2)}) copy-start(bf16[128,512]{0,1:T(8,128)(2,1)} %copy.178) | copy-start | bytes 393220
  210.9 3.9 %copy-start.23 = (f32[128,128,2]{1,0,2:T(8,128)S(1)}, f32[128,128,2]{1,0,2:T(8,128)}, u32[]{:S(2)}) copy-start(f32[128,128,2]{1,0,2:T(8,128)} %copy.181) | copy-start | bytes 393220
  210.9 3.9 %copy-start.40 = (f32[128,8]{0,1:T(8,128)S(1)}, f32[128,8]{0,1:T(8,128)}, u32[]{:S(2)}) copy-start(f32[128,8]{0,1:T(8,128)} %rev.22) | copy-start | bytes 12292
  210.9 3.9 %copy-start.49 = (f32[128,2,4]{0,2,1:T(4,128)S(1)}, f32[128,2,4]{0,2,1:T(4,128)}, u32[]{:S(2)}) copy-start(f32[128,2,4]{0,2,1:T(4,128)} %copy.183) | copy-start | bytes 12292
  213.7 8.4 %copy-start.4 = (f32[2,4,64,64]{3,2,1,0:T(8,128)S(1)}, f32[2,4,64,64]{3,2,1,0:T(8,128)}, u32[]{:S(2)}) copy-start(f32[2,4,64,64]{3,2,1,0:T(8,128)} %copy-done.3) | copy-start | bytes 393220
  220.9 3.9 %copy-start.8 = (f32[128,512]{0,1:T(8,128)S(1)}, f32[128,512]{0,1:T(8,128)}, u32[]{:S(2)}) copy-start(f32[128,512]{0,1:T(8,128)} %copy.190) | copy-start | bytes 786436
  220.9 3.9 %copy-start.9 = (f32[128,2,4,64]{0,3,2,1:T(8,128)S(1)}, f32[128,2,4,64]{0,3,2,1:T(8,128)}, u32[]{:S(2)}) copy-start(f32[128,2,4,64]{0,3,2,1:T(8,128)} %rev.23) | copy-start | bytes 786436
  220.9 3.9 %copy-start.17 = (f32[128,128,2]{1,0,2:T(8,128)S(1)}, f32[128,128,2]{1,0,2:T(8,128)}, u32[]{:S(2)}) copy-start(f32[128,128,2]{1,0,2:T(8,128)} %copy.168) | copy-start | bytes 393220
  220.9 3.9 %copy-start.26 = (f32[128,8]{0,1:T(8,128)S(1)}, f32[128,8]{0,1:T(8,128)}, u32[]{:S(2)}) copy-start(f32[128,8]{0,1:T(8,128)} %copy-done.25) | copy-start | bytes 12292
  220.9 3.9 %copy-start.29 = (f32[128,2,4]{0,2,1:T(4,128)S(1)}, f32[128,2,4]{0,2,1:T(4,128)}, u32[]{:S(2)}) copy-start(f32[128,2,4]{0,2,1:T(4,128)} %copy.170) | copy-start | bytes 12292
  222.0 3.2 %copy-start.35 = (f32[2,4,64]{2,1,0:T(4,128)S(1)}, f32[2,4,64]{2,1,0:T(4,128)}, u32[]{:S(2)}) copy-start(f32[2,4,64]{2,1,0:T(4,128)} %reshape.218) | copy-start | bytes 6148
  224.8 9.5 %copy-start.7 = (bf16[64,2048]{1,0:T(8,128)(2,1)S(1)}, bf16[64,2048]{1,0:T(8,128)(2,1)}, u32[]{:S(2)}) copy-start(bf16[64,2048]{1,0:T(8,128)(2,1)} %param.22) | copy-start | bytes 786436
  225.2 9.1 %copy-start.30 = (f32[1,2048]{1,0:T(1,128)S(1)}, f32[1,2048]{1,0:T(1,128)}, u32[]{:S(2)}) copy-start(f32[1,2048]{1,0:T(1,128)} %get-tuple-element.226) | copy-start | bytes 24580
